TPU v7x, 32 devices: a whole 2x2x4 slice. The times are simulated.
32 devices in a mesh: grp: 2 (over y), sp: 4 (over z), fs: 2 (over x), tp: 2 (over core).
Axes of the slice: x: 2, y: 2, z: 4, core: 2. Of those that a mesh axis runs over, the one named last changes fastest.
Arguments:
- tokens: bfloat16 [4, 512, 2048], P(('grp', 'fs'), 'sp', 'tp'), parts along dimension 0, may hold values from -120 to 120
- mix_gain: float32 [2048], replicated, may hold values from 0.1 to 1.9
- attn_query: bfloat16 [2048, 1024], P('fs', 'tp'), may hold values from -0.375 to 0.375
- attn_key: bfloat16 [2048, 1024], P('fs', 'tp'), may hold values from -0.125 to 0.125
- attn_value: bfloat16 [2048, 1024], P('fs', 'tp'), may hold values from -0.125 to 0.125
- rec_query: bfloat16 [2048, 1024], P('fs', 'tp'), may hold values from -0.125 to 0.125
- rec_forget: bfloat16 [2048, 1024], P('fs', 'tp'), may hold values from -0.125 to 0.125
- rec_input: bfloat16 [2048, 1024], P('fs', 'tp'), may hold values from -0.125 to 0.125
- break_offset: float32 [8], P('tp'), may hold values from -13.5 to -7
- forget_room: float32 [8, 128], P('tp'), may hold values from 0.0009765625 to 0.05
- out_gain: float32 [128], replicated, may hold values from 0.1 to 1.9
- out_attn: bfloat16 [1024, 2048], P('tp', 'fs'), may hold values from -0.125 to 0.125
- out_rec: bfloat16 [1024, 2048], P('tp', 'fs'), may hold values from -0.125 to 0.125
Outputs:
- mixed: bfloat16 [4, 512, 2048], P(('grp', 'fs'), ('sp', 'tp')), parts along dimension 0
There are 2 independent parts, one for each index of `grp`. A program takes and returns all parts, laid end to end along the dimension named above; an argument that names none is the same for every part. Nothing has to cross between parts.
All inputs are finite; a program needn't handle non-finite values.
Results may differ from a plain program's by a relative error of at most 0.019.
Values may be sent and summed in bfloat16 or wider, within the bound.
A program may use at most 64 MiB of HBM per device.

v0:
```python
import math
import jax
import jax.numpy as jnp
from jax import lax
from jax.sharding import PartitionSpec as P

HEAD = 128
DK = 128
DV = 128
REC_BLOCK = 64
norm_eps = 1e-06
highest = lax.Precision.HIGHEST


def carried_in(x, axis, join, neutral):
    place = lax.axis_index(axis)
    gathered = jax.tree.map(
        lambda a, kind: lax.all_gather(a.astype(kind), axis), x, (jnp.bfloat16, jnp.bfloat16)
    )
    state = jax.tree.map(lambda a, e: jnp.zeros_like(a) + jnp.asarray(e, a.dtype), x, neutral)

    def one(step, state):
        return join(
            state,
            jax.tree.map(
                lambda a, own: lax.dynamic_index_in_dim(a, step, 0, False).astype(own.dtype),
                gathered,
                x,
            ),
        )

    return lax.fori_loop(0, place, one, state)


def block_step(states, inputs):
    queries, key_in, value_rows, log_forget = inputs
    block_len = queries.shape[-2]
    cum_log = jnp.cumsum(log_forget, axis=-2)
    last_log = cum_log[..., -1:, :]
    q_dec = queries * jnp.exp(cum_log)
    k_inv = key_in * jnp.exp(-cum_log)
    causal = lax.iota(jnp.int32, block_len)[:, None] >= lax.iota(jnp.int32, block_len)[None, :]
    carried_part = jnp.einsum("...tk,...kv->...tv", q_dec, states, precision=highest)
    scores = jnp.where(
        causal, jnp.einsum("...tk,...sk->...ts", q_dec, k_inv, precision=highest), 0.0
    )
    inner_part = jnp.einsum("...ts,...sv->...tv", scores, value_rows, precision=highest)
    fresh_state = jnp.einsum(
        "...sk,...sv->...kv", key_in * jnp.exp(last_log - cum_log), value_rows, precision=highest
    )
    return (
        jnp.exp(jnp.swapaxes(last_log, -1, -2)) * states + fresh_state,
        carried_part + inner_part,
    )


def stick_mixer(queries, key_rows, value_rows, offsets):
    seq_count, tok_rows, head_count, head_width = queries.shape
    own_index = lax.axis_index("sp")
    sp_count = lax.axis_size("sp")
    factor = 1.0 / math.sqrt(head_width)
    q_pos = own_index * tok_rows + lax.iota(jnp.int32, tok_rows)
    start_acc = jnp.zeros((sp_count, seq_count, tok_rows, head_count, head_width), jnp.float32)
    start_log = jnp.zeros((sp_count, seq_count, tok_rows, head_count), jnp.float32)

    def one_block(carried, key_blk, value_blk, slot):

        def compute(states):
            sums_acc, log_sums = states
            scores = jnp.einsum(
                "bqhe,bkhe->bhqk", queries, key_blk, preferred_element_type=jnp.float32
            )
            scores = scores * factor + offsets[None, :, None, None]
            k_pos = slot * tok_rows + lax.iota(jnp.int32, tok_rows)
            strict = k_pos[None, :] < q_pos[:, None]
            log_keep = jnp.where(strict, jax.nn.log_sigmoid(-scores), 0.0)
            inner_sum = lax.cumsum(log_keep, axis=3, reverse=True) - log_keep
            sticks = jnp.where(strict, jnp.exp(jax.nn.log_sigmoid(scores) + inner_sum), 0.0).astype(
                jnp.bfloat16
            )
            partial_value = jnp.einsum(
                "bhqk,bkhe->bqhe", sticks, value_blk, preferred_element_type=jnp.float32
            )
            totals = jnp.transpose(jnp.sum(log_keep, axis=3), (0, 2, 1))
            return (
                lax.dynamic_update_index_in_dim(sums_acc, partial_value, slot, 0),
                lax.dynamic_update_index_in_dim(log_sums, totals, slot, 0),
            )

        return lax.cond(slot <= own_index, compute, lambda states: states, carried)

    key_all = lax.all_gather(key_rows, "sp", axis=1, tiled=True)
    value_all = lax.all_gather(value_rows, "sp", axis=1, tiled=True)
    blocks = key_all.shape[1] // tok_rows

    def turn(block_idx, states):
        key_blk = lax.dynamic_slice_in_dim(key_all, block_idx * tok_rows, tok_rows, 1)
        value_blk = lax.dynamic_slice_in_dim(value_all, block_idx * tok_rows, tok_rows, 1)
        return one_block(states, key_blk, value_blk, block_idx)

    sums_acc, log_sums = lax.fori_loop(0, blocks, turn, (start_acc, start_log))
    later_sum = jnp.cumsum(log_sums[::-1], axis=0)[::-1] - log_sums
    return jnp.sum(sums_acc * jnp.exp(later_sum)[..., None], axis=0).astype(jnp.bfloat16)


def combine_states(earlier, later):
    return (earlier[0] + later[0], jnp.exp(later[0])[..., None] * earlier[1] + later[1])


def recur_mixer(queries, gate_pre, inputs, rooms, gain):
    seq_count, tok_rows, head_count, key_dim = queries.shape
    val_dim = inputs.shape[3]
    key_in = rooms * jax.nn.sigmoid(-gate_pre.astype(jnp.float32))
    log_forget = jnp.log1p(-key_in)
    query32 = queries.astype(jnp.float32)
    blocks = tok_rows // REC_BLOCK

    def split_blocks(tensor):
        return jnp.transpose(
            tensor.reshape(seq_count, blocks, REC_BLOCK, head_count, tensor.shape[3]),
            (1, 0, 3, 2, 4),
        )

    empty_state = jnp.zeros((seq_count, head_count, key_dim, val_dim), jnp.float32)
    final_state, pieces = lax.scan(
        block_step,
        empty_state,
        (
            split_blocks(query32),
            split_blocks(key_in),
            split_blocks(inputs.astype(jnp.float32)),
            split_blocks(log_forget),
        ),
    )
    local_out = jnp.transpose(pieces, (1, 0, 3, 2, 4)).reshape(
        seq_count, tok_rows, head_count, val_dim
    )
    running = jnp.cumsum(log_forget, axis=1)
    identity = (jnp.zeros((seq_count, head_count, key_dim), jnp.float32), empty_state)
    incoming = carried_in((running[:, -1], final_state), "sp", combine_states, identity)[1]
    raw_out = local_out + jnp.einsum(
        "bthk,bhkv->bthv", query32 * jnp.exp(running), incoming, precision=highest
    )
    factor = lax.rsqrt(jnp.mean(raw_out * raw_out, axis=3, keepdims=True) + norm_eps)
    return (raw_out * factor * gain).astype(jnp.bfloat16)


def body(
    tokens,
    mix_gain,
    attn_query,
    attn_key,
    attn_value,
    rec_query,
    rec_forget,
    rec_input,
    break_offset,
    forget_room,
    out_gain,
    out_attn,
    out_rec,
):
    whole = lax.all_gather(tokens, "tp", axis=2, tiled=True)
    seq_rows = whole.shape[1]
    model_width = whole.shape[2]
    rows32 = whole.astype(jnp.float32)
    factor = lax.rsqrt(jnp.mean(rows32 * rows32, axis=2, keepdims=True) + norm_eps)
    normed = (rows32 * factor * mix_gain).astype(jnp.bfloat16).reshape(seq_rows, model_width)
    weights = (attn_query, attn_key, attn_value, rec_query, rec_forget, rec_input)
    turned = (
        lax.all_to_all(weights[0], "fs", split_axis=1, concat_axis=0, tiled=True),
        lax.all_to_all(weights[1], "fs", split_axis=1, concat_axis=0, tiled=True),
        lax.all_to_all(weights[2], "fs", split_axis=1, concat_axis=0, tiled=True),
        lax.all_to_all(weights[3], "fs", split_axis=1, concat_axis=0, tiled=True),
        lax.all_to_all(weights[4], "fs", split_axis=1, concat_axis=0, tiled=True),
        lax.all_to_all(weights[5], "fs", split_axis=1, concat_axis=0, tiled=True),
    )
    pieces = lax.all_gather(normed, "fs", axis=0, tiled=True)
    projected = tuple(
        (
            jnp.dot(pieces, matrix, preferred_element_type=jnp.float32).astype(jnp.bfloat16)
            for matrix in turned
        )
    )
    seq_count = lax.axis_size("fs")
    own_fs = lax.axis_index("fs")
    attn_heads = break_offset.shape[0] // seq_count
    rec_heads = forget_room.shape[0] // seq_count
    offsets = lax.dynamic_slice_in_dim(break_offset, own_fs * attn_heads, attn_heads, 0)
    rooms = lax.dynamic_slice_in_dim(forget_room, own_fs * rec_heads, rec_heads, 0)

    def heads_of(matrix, width_each):
        return matrix.reshape(seq_count, seq_rows, matrix.shape[1] // width_each, width_each)

    attn_out = stick_mixer(
        heads_of(projected[0], HEAD),
        heads_of(projected[1], HEAD),
        heads_of(projected[2], HEAD),
        offsets,
    )
    rec_out = recur_mixer(
        heads_of(projected[3], DK),
        heads_of(projected[4], DK),
        heads_of(projected[5], DV),
        rooms,
        out_gain,
    )
    attn_flat = attn_out.reshape(seq_count * seq_rows, -1)
    rec_flat = rec_out.reshape(seq_count * seq_rows, -1)
    attn_flat, rec_flat = (
        lax.all_to_all(attn_flat, "fs", split_axis=0, concat_axis=1, tiled=True),
        lax.all_to_all(rec_flat, "fs", split_axis=0, concat_axis=1, tiled=True),
    )
    full_attn, full_rec = (
        lax.all_gather(out_attn, "fs", axis=1, tiled=True),
        lax.all_gather(out_rec, "fs", axis=1, tiled=True),
    )
    share = seq_rows // lax.axis_size("tp")
    mixed = lax.psum_scatter(
        (
            jnp.dot(attn_flat, full_attn, preferred_element_type=jnp.float32)
            + jnp.dot(rec_flat, full_rec, preferred_element_type=jnp.float32)
        ).astype(jnp.bfloat16),
        "tp",
        scatter_dimension=0,
        tiled=True,
    )
    return mixed.reshape(1, share, model_width)


def solution(mesh):
    placed = (
        P(("grp", "fs"), "sp", "tp"),
        P(),
        P("fs", "tp"),
        P("fs", "tp"),
        P("fs", "tp"),
        P("fs", "tp"),
        P("fs", "tp"),
        P("fs", "tp"),
        P("tp"),
        P("tp", None),
        P(),
        P("tp", "fs"),
        P("tp", "fs"),
    )
    return jax.shard_map(
        body,
        mesh=mesh,
        in_specs=placed,
        out_specs=P(("grp", "fs"), ("sp", "tp"), None),
        check_vma=False,
    )
```

profile of v0, /device:TPU:0, one launch (start us, length us, event | category | flops | bytes accessed | tf_op | source)
XLA Modules:
  0.0 285.6 jit_solution(8007163119693888808)
XLA Ops:
  12.4 4.1 %all-to-all-start.4 = ((bf16[1024,2,256]{0,2,1:T(8,128)(2,1)}), bf16[1024,2,256]{0,2,1:T(8,128)(2,1)S(1)}, u32[]{:S(2)}, u32[]{:S(2)}) async-start(bf16[1024,2,256]{0,2,1:T(8,128)(2,1)} %bitcast.20), calls=%async_computation.4 | async-start | bytes 2097152 | tf_op jit(solution)/shard_map/all_to_all | solution.py:175
  17.9 21.6 %all-to-all-done.4 = bf16[1024,2,256]{0,2,1:T(8,128)(2,1)S(1)} async-done(((bf16[1024,2,256]{0,2,1:T(8,128)(2,1)}), bf16[1024,2,256]{0,2,1:T(8,128)(2,1)S(1)}, u32[]{:S(2)}, u32[]{:S(2)}) %all-to-all-start.4) | async-done | bytes 1048608 | tf_op jit(solution)/shard_map/all_to_all | solution.py:175
  39.4 3.6 %all-to-all-start.6 = ((bf16[1024,2,256]{0,2,1:T(8,128)(2,1)}), bf16[1024,2,256]{0,2,1:T(8,128)(2,1)S(1)}, u32[]{:S(2)}, u32[]{:S(2)}) async-start(bf16[1024,2,256]{0,2,1:T(8,128)(2,1)} %bitcast.29), calls=%async_computation.6 | async-start | bytes 2097152 | tf_op jit(solution)/shard_map/all_to_all | solution.py:174
  45.1 10.5 %all-to-all-done.6 = bf16[1024,2,256]{0,2,1:T(8,128)(2,1)S(1)} async-done(((bf16[1024,2,256]{0,2,1:T(8,128)(2,1)}), bf16[1024,2,256]{0,2,1:T(8,128)(2,1)S(1)}, u32[]{:S(2)}, u32[]{:S(2)}) %all-to-all-start.6) | async-done | bytes 1048608 | tf_op jit(solution)/shard_map/all_to_all | solution.py:174
  55.6 3.6 %all-to-all-start.5 = ((bf16[1024,2,256]{0,2,1:T(8,128)(2,1)}), bf16[1024,2,256]{0,2,1:T(8,128)(2,1)S(1)}, u32[]{:S(2)}, u32[]{:S(2)}) async-start(bf16[1024,2,256]{0,2,1:T(8,128)(2,1)} %bitcast.144), calls=%async_computation.5 | async-start | bytes 2097152 | tf_op jit(solution)/shard_map/all_to_all | solution.py:176
  61.5 22.8 %all-to-all-done.5 = bf16[1024,2,256]{0,2,1:T(8,128)(2,1)S(1)} async-done(((bf16[1024,2,256]{0,2,1:T(8,128)(2,1)}), bf16[1024,2,256]{0,2,1:T(8,128)(2,1)S(1)}, u32[]{:S(2)}, u32[]{:S(2)}) %all-to-all-start.5) | async-done | bytes 1048608 | tf_op jit(solution)/shard_map/all_to_all | solution.py:176
  84.3 4.4 %all-to-all-start = ((bf16[1024,2,256]{0,2,1:T(8,128)(2,1)}), bf16[1024,2,256]{0,2,1:T(8,128)(2,1)}, u32[]{:S(2)}, u32[]{:S(2)}) async-start(bf16[1024,2,256]{0,2,1:T(8,128)(2,1)} %bitcast.145), calls=%async_computation | async-start | bytes 2097152 | tf_op jit(solution)/shard_map/all_to_all | solution.py:172
  91.1 12.6 %all-to-all-done = bf16[1024,2,256]{0,2,1:T(8,128)(2,1)} async-done(((bf16[1024,2,256]{0,2,1:T(8,128)(2,1)}), bf16[1024,2,256]{0,2,1:T(8,128)(2,1)}, u32[]{:S(2)}, u32[]{:S(2)}) %all-to-all-start) | async-done | bytes 1048608 | tf_op jit(solution)/shard_map/all_to_all | solution.py:172
  103.7 4.5 %all-to-all-start.2 = ((bf16[1024,2,256]{0,2,1:T(8,128)(2,1)}), bf16[1024,2,256]{0,2,1:T(8,128)(2,1)}, u32[]{:S(2)}, u32[]{:S(2)}) async-start(bf16[1024,2,256]{0,2,1:T(8,128)(2,1)} %bitcast.146), calls=%async_computation.2 | async-start | bytes 2097152 | tf_op jit(solution)/shard_map/all_to_all | solution.py:173
  110.4 10.6 %all-to-all-done.2 = bf16[1024,2,256]{0,2,1:T(8,128)(2,1)} async-done(((bf16[1024,2,256]{0,2,1:T(8,128)(2,1)}), bf16[1024,2,256]{0,2,1:T(8,128)(2,1)}, u32[]{:S(2)}, u32[]{:S(2)}) %all-to-all-start.2) | async-done | bytes 1048608 | tf_op jit(solution)/shard_map/all_to_all | solution.py:173
  121.1 4.4 %all-to-all-start.1 = ((bf16[1024,2,256]{0,2,1:T(8,128)(2,1)}), bf16[1024,2,256]{0,2,1:T(8,128)(2,1)}, u32[]{:S(2)}, u32[]{:S(2)}) async-start(bf16[1024,2,256]{0,2,1:T(8,128)(2,1)} %bitcast.141), calls=%async_computation.1 | async-start | bytes 2097152 | tf_op jit(solution)/shard_map/all_to_all | solution.py:171
  156.2 6.9 %while.43 = (s32[]{:T(128)}, f32[2,2,128,128]{3,2,1,0:T(8,128)S(1)}, f32[2,2,2,64,128]{4,3,0,2,1:T(8,128)}, f32[2,2,2,64,128]{4,3,2,1,0:T(8,128)}, f32[2,2,2,64,...) while((s32[]{:T(128)}, ...), condition=%wide.region_11.12_spmd.clone, body=%wide.region_9.11_spmd.clone.sunk | while | flops 153571328 | bytes 3239036 | solution.py:125
  163.1 16.6 %all-gather.2 = bf16[8,2,128,128]{3,2,1,0:T(8,128)(2,1)} all-gather(bf16[2,2,128,128]{3,2,1,0:T(8,128)(2,1)S(1)} %convert_element_type.118), channel_id=4, replica_groups=mesh['grp'=2,'sp'=4,'fs'=2,'tp'=2] {'sp'}, dimensions={0}, use_global_device_ids=true | all-gather | bytes 655360 | tf_op jit(solution)/shard_map/all_gather | solution.py:18
  182.0 9.4 %all-gather.1 = bf16[8,1,2,128]{3,2,1,0:T(2,128)(2,1)S(1)} all-gather(bf16[2,1,2,128]{3,2,1,0:T(2,128)(2,1)S(1)} %slice.12), channel_id=3, replica_groups=mesh['grp'=2,'sp'=4,'fs'=2,'tp'=2] {'sp'}, dimensions={0}, use_global_device_ids=true | all-gather | bytes 5120 | tf_op jit(solution)/shard_map/all_gather | solution.py:18
  195.0 16.5 %all_gather.30 = bf16[2,512,2,128]{3,1,2,0:T(8,128)(2,1)} all-gather(bf16[2,128,2,128]{3,1,2,0:T(8,128)(2,1)S(1)} %copy.84), channel_id=1, replica_groups=mesh['grp'=2,'sp'=4,'fs'=2,'tp'=2] {'sp'}, dimensions={1}, use_global_device_ids=true | all-gather | bytes 655360 | tf_op jit(solution)/shard_map/all_gather | solution.py:92
  212.1 14.9 %all_gather.31 = bf16[2,512,2,128]{3,1,2,0:T(8,128)(2,1)S(1)} all-gather(bf16[2,128,2,128]{3,1,2,0:T(8,128)(2,1)S(1)} %copy.89), channel_id=1, replica_groups=mesh['grp'=2,'sp'=4,'fs'=2,'tp'=2] {'sp'}, dimensions={1}, use_global_device_ids=true | all-gather | bytes 655360 | tf_op jit(solution)/shard_map/all_gather | solution.py:93
  227.6 6.6 %while.42 = (s32[]{:T(128)}, f32[4,2,128,2,128]{4,2,3,1,0:T(8,128)S(1)}, f32[4,2,128,2]{2,3,1,0:T(2,128)S(1)}, s32[]{:T(128)}, bf16[2,512,2,128]{3,1,2,0:T(8,128...) while((s32[]{:T(128)}, ...), condition=%wide.region_6.7_spmd.clone, body=%wide.region_1.6_spmd.clone.sunk | while | flops 43925260 | bytes 2286935 | solution.py:101
  227.7 6.4 %conditional.3 = ((f32[4,2,128,2,128]{4,2,3,1,0:T(8,128)S(1)}, f32[4,2,128,2]{2,3,1,0:T(2,128)S(1)})) conditional(s32[]{:T(128)} %convert_element_type.168, (f32[4,2,128,2,128]{4,2,3,1,0:T(8,128)S(1)}, f32[4,2,128,2]{2,3,1,0:T(2,128)S(1)}) %tuple.100, (s32[]{:T(128)}, s32[]{:T(128)}, bf16[2,512,2,128]{3,1,2,0:T(8,128)(2,1)}, ...), branch_computations={%region_2.0_spmd, %region_3.5_spmd} | conditional | flops 43925256 | bytes 2286220 | solution.py:90
  229.1 4.4 %reduce_window_sum.43 = f32[2,2,128,128]{2,3,1,0:T(8,128)S(1)} reduce-window(f32[2,2,128,128]{2,3,1,0:T(8,128)S(1)} %get-tuple-element.514, f32[]{:T(128)} %constant.131.clone), window={size=1x1x1x128 pad=0_0x0_0x0_0x0_127}, to_apply=%region_4.3 | reduce-window | flops 8323072 | bytes 524292 | tf_op jit(solution)/shard_map/while/body/eval_jaxpr/cond/branch_1_fun/reduce_window_sum | solution.py:77
  235.5 3.4 %all-to-all-start.3 = ((bf16[2,128,256]{1,2,0:T(8,128)(2,1)}), bf16[2,128,256]{1,2,0:T(8,128)(2,1)S(1)}, u32[]{:S(2)}, u32[]{:S(2)}) async-start(bf16[2,128,256]{1,2,0:T(8,128)(2,1)} %bitcast.17), calls=%async_computation.3 | async-start | bytes 262144 | tf_op jit(solution)/shard_map/all_to_all | solution.py:211
  240.3 3.0 %all-to-all-done.3 = bf16[2,128,256]{1,2,0:T(8,128)(2,1)S(1)} async-done(((bf16[2,128,256]{1,2,0:T(8,128)(2,1)}), bf16[2,128,256]{1,2,0:T(8,128)(2,1)S(1)}, u32[]{:S(2)}, u32[]{:S(2)}) %all-to-all-start.3) | async-done | bytes 131104 | tf_op jit(solution)/shard_map/all_to_all | solution.py:211
  243.3 3.4 %all-to-all-start.7 = ((bf16[2,128,256]{1,2,0:T(8,128)(2,1)}), bf16[2,128,256]{1,2,0:T(8,128)(2,1)S(1)}, u32[]{:S(2)}, u32[]{:S(2)}) async-start(bf16[2,128,256]{1,2,0:T(8,128)(2,1)} %bitcast.38), calls=%async_computation.7 | async-start | bytes 262144 | tf_op jit(solution)/shard_map/all_to_all | solution.py:212
  251.1 2.9 %fusion.44 = bf16[128,2048]{1,0:T(8,128)(2,1)} fusion(f32[128,2048]{1,0:T(8,128)S(1)} %fusion.69, bf16[128,512]{0,1:T(8,128)(2,1)S(1)} %bitcast.150, bf16[512,2048]{1,0:T(8,128)(2,1)} %all-gather.9.cloned.1.call-done), kind=kOutput, calls=%fused_computation.60 | convolution fusion | flops 268959744 | bytes 3801088 | tf_op jit(solution)/shard_map/dot_general | solution.py:222
  254.0 25.0 %reduce-scatter.2.cloned.1.call-done = bf16[64,2048]{1,0:T(8,128)(2,1)} async-done(((bf16[128,2048]{1,0:T(8,128)(2,1)}), bf16[64,2048]{1,0:T(8,128)(2,1)}) %reduce-scatter.2.cloned.1.call-update) | async-done | bytes 262160 | tf_op jit(solution)/shard_map/reduce_scatter | solution.py:219
  (123 shorter events, 69.5 us)
Async XLA Ops:
  6.5 119.8 %copy-start = (f32[4,128]{1,0:T(4,128)S(1)}, f32[4,128]{1,0:T(4,128)}, u32[]{:S(2)}) copy-start(f32[4,128]{1,0:T(4,128)} %param.30) | copy-start | bytes 6148
  6.5 4.5 %copy-start.4 = (bf16[1024,512]{1,0:T(8,128)(2,1)S(1)}, bf16[1024,512]{1,0:T(8,128)(2,1)}, u32[]{:S(2)}) copy-start(bf16[1024,512]{1,0:T(8,128)(2,1)} %param.27) | copy-start | bytes 3145732
  6.5 132.5 %all-gather.11.cloned.1.call-start = ((), (), s32[]{:S(2)}) async-start(), calls=%async_computation.12 | async-start | bytes 1572864 | tf_op jit(solution)/shard_map/all_gather | solution.py:178
  11.1 5.5 %copy-start.5 = (bf16[1024,512]{1,0:T(8,128)(2,1)S(1)}, bf16[1024,512]{1,0:T(8,128)(2,1)}, u32[]{:S(2)}) copy-start(bf16[1024,512]{1,0:T(8,128)(2,1)} %param.26) | copy-start | bytes 3145732
  12.4 27.0 %all-to-all-start.4 = ((bf16[1024,2,256]{0,2,1:T(8,128)(2,1)}), bf16[1024,2,256]{0,2,1:T(8,128)(2,1)S(1)}, u32[]{:S(2)}, u32[]{:S(2)}) async-start(bf16[1024,2,256]{0,2,1:T(8,128)(2,1)} %bitcast.20), calls=%async_computation.4 | async-start | bytes 2097152 | tf_op jit(solution)/shard_map/all_to_all | solution.py:175
  17.9 25.9 %copy-start.6 = (bf16[1024,512]{1,0:T(8,128)(2,1)S(1)}, bf16[1024,512]{1,0:T(8,128)(2,1)}, u32[]{:S(2)}) copy-start(bf16[1024,512]{1,0:T(8,128)(2,1)} %param.28) | copy-start | bytes 3145732
  39.4 16.2 %all-to-all-start.6 = ((bf16[1024,2,256]{0,2,1:T(8,128)(2,1)}), bf16[1024,2,256]{0,2,1:T(8,128)(2,1)S(1)}, u32[]{:S(2)}, u32[]{:S(2)}) async-start(bf16[1024,2,256]{0,2,1:T(8,128)(2,1)} %bitcast.29), calls=%async_computation.6 | async-start | bytes 2097152 | tf_op jit(solution)/shard_map/all_to_all | solution.py:174
  43.0 203.7 %all-gather.7.cloned.1.call-start = ((), (), s32[]{:S(2)}) async-start(), calls=%async_computation.9 | async-start | bytes 3145728 | tf_op jit(solution)/shard_map/all_gather | solution.py:215
  55.6 28.7 %all-to-all-start.5 = ((bf16[1024,2,256]{0,2,1:T(8,128)(2,1)}), bf16[1024,2,256]{0,2,1:T(8,128)(2,1)S(1)}, u32[]{:S(2)}, u32[]{:S(2)}) async-start(bf16[1024,2,256]{0,2,1:T(8,128)(2,1)} %bitcast.144), calls=%async_computation.5 | async-start | bytes 2097152 | tf_op jit(solution)/shard_map/all_to_all | solution.py:176
  84.3 19.3 %all-to-all-start = ((bf16[1024,2,256]{0,2,1:T(8,128)(2,1)}), bf16[1024,2,256]{0,2,1:T(8,128)(2,1)}, u32[]{:S(2)}, u32[]{:S(2)}) async-start(bf16[1024,2,256]{0,2,1:T(8,128)(2,1)} %bitcast.145), calls=%async_computation | async-start | bytes 2097152 | tf_op jit(solution)/shard_map/all_to_all | solution.py:172
  103.7 17.4 %all-to-all-start.2 = ((bf16[1024,2,256]{0,2,1:T(8,128)(2,1)}), bf16[1024,2,256]{0,2,1:T(8,128)(2,1)}, u32[]{:S(2)}, u32[]{:S(2)}) async-start(bf16[1024,2,256]{0,2,1:T(8,128)(2,1)} %bitcast.146), calls=%async_computation.2 | async-start | bytes 2097152 | tf_op jit(solution)/shard_map/all_to_all | solution.py:173
  110.4 15.8 %copy-start.11 = (f32[4]{0:T(128)S(1)}, f32[4]{0:T(128)}, u32[]{:S(2)}) copy-start(f32[4]{0:T(128)} %param.29) | copy-start | bytes 52
  121.1 16.5 %all-to-all-start.1 = ((bf16[1024,2,256]{0,2,1:T(8,128)(2,1)}), bf16[1024,2,256]{0,2,1:T(8,128)(2,1)}, u32[]{:S(2)}, u32[]{:S(2)}) async-start(bf16[1024,2,256]{0,2,1:T(8,128)(2,1)} %bitcast.141), calls=%async_computation.1 | async-start | bytes 2097152 | tf_op jit(solution)/shard_map/all_to_all | solution.py:171
  125.5 125.7 %all-gather.9.cloned.1.call-start = ((), (), s32[]{:S(2)}) async-start(), calls=%async_computation.10 | async-start | bytes 3145728 | tf_op jit(solution)/shard_map/all_gather | solution.py:216
  132.6 6.5 %copy-start.7 = (bf16[2,1024,256]{2,1,0:T(8,128)(2,1)S(1)}, bf16[2,1024,256]{2,1,0:T(8,128)(2,1)}, u32[]{:S(2)}) copy-start(bf16[2,1024,256]{2,1,0:T(8,128)(2,1)} %copy.93) | copy-start | bytes 3145732
  139.1 6.2 %copy-start.1 = (bf16[1,256,2048]{2,1,0:T(8,128)(2,1)S(1)}, bf16[1,256,2048]{2,1,0:T(8,128)(2,1)}, u32[]{:S(2)}) copy-start(bf16[1,256,2048]{2,1,0:T(8,128)(2,1)} %all-gather.11.cloned.1.call-done) | copy-start | bytes 3145732
  143.4 7.8 %copy-start.3 = (bf16[2,1024,256]{2,1,0:T(8,128)(2,1)S(1)}, bf16[2,1024,256]{2,1,0:T(8,128)(2,1)}, u32[]{:S(2)}) copy-start(bf16[2,1024,256]{2,1,0:T(8,128)(2,1)} %copy.96) | copy-start | bytes 3145732
  182.0 29.5 %copy-start.2 = (bf16[2,1024,256]{2,1,0:T(8,128)(2,1)S(1)}, bf16[2,1024,256]{2,1,0:T(8,128)(2,1)}, u32[]{:S(2)}) copy-start(bf16[2,1024,256]{2,1,0:T(8,128)(2,1)} %copy.88) | copy-start | bytes 3145732
  234.7 4.2 %copy-start.8 = (f32[2,128,2,128]{1,3,2,0:T(8,128)S(1)}, f32[2,128,2,128]{1,3,2,0:T(8,128)}, u32[]{:S(2)}) copy-start(f32[2,128,2,128]{1,3,2,0:T(8,128)} %copy.104) | copy-start | bytes 786436
  234.7 4.2 %copy-start.9 = (f32[2,128,2,128]{3,2,1,0:T(2,128)S(1)}, f32[2,128,2,128]{3,2,1,0:T(2,128)}, u32[]{:S(2)}) copy-start(f32[2,128,2,128]{3,2,1,0:T(2,128)} %get-tuple-element.520) | copy-start | bytes 786436
  235.5 7.8 %all-to-all-start.3 = ((bf16[2,128,256]{1,2,0:T(8,128)(2,1)}), bf16[2,128,256]{1,2,0:T(8,128)(2,1)S(1)}, u32[]{:S(2)}, u32[]{:S(2)}) async-start(bf16[2,128,256]{1,2,0:T(8,128)(2,1)} %bitcast.17), calls=%async_computation.3 | async-start | bytes 262144 | tf_op jit(solution)/shard_map/all_to_all | solution.py:211
  238.9 0.7 copy-start.10
  243.3 7.8 %all-to-all-start.7 = ((bf16[2,128,256]{1,2,0:T(8,128)(2,1)}), bf16[2,128,256]{1,2,0:T(8,128)(2,1)S(1)}, u32[]{:S(2)}, u32[]{:S(2)}) async-start(bf16[2,128,256]{1,2,0:T(8,128)(2,1)} %bitcast.38), calls=%async_computation.7 | async-start | bytes 262144 | tf_op jit(solution)/shard_map/all_to_all | solution.py:212
  246.7 32.4 %reduce-scatter.2.cloned.1.call-start = ((), (), s32[]{:S(2)}) async-start(), calls=%async_computation.11 | async-start | bytes 786432 | tf_op jit(solution)/shard_map/reduce_scatter | solution.py:219
Sparse Core Ops, SparseCore 0:
  11.2 31.5 all-gather.10
  45.4 49.9 all-gather.6
  127.8 34.1 all-gather.8
  254.2 24.8 reduce-scatter.1
where the time goes:
time: 287 us; the launch traced here: 286 us
  waiting for transfers between devices  112 us (39%)
  blocking collectives  60.2 us (21%)
  local copies, waits for them, and re-layouts  35.2 us (12%)
  starting transfers between devices  31.5 us (11%)
  matrix products  20.6 us (7%)
  between operations  13.5 us (5%)
  other arithmetic  11.9 us (4%)
    all_gather x2, blocking collectives, carried_in(): lax.all_gather(a.astype(kind), axis)  26.1 us
    reduce_scatter x1, waiting for transfers between devices, body(): lax.psum_scatter((jnp.dot(attn_flat, full_attn, preferred_element_type=jn...  25 us
    all_to_all x1, waiting for transfers between devices, body(): lax.all_to_all(weights[5], 'fs', split_axis=1, concat_axis=0, tiled=True)  22.8 us
    all_to_all x1, waiting for transfers between devices, body(): lax.all_to_all(weights[4], 'fs', split_axis=1, concat_axis=0, tiled=True)  21.6 us
    all_gather x1, blocking collectives, stick_mixer(): key_all = lax.all_gather(key_rows, 'sp', axis=1, tiled=True)  16.5 us
    all_gather x1, blocking collectives, stick_mixer(): value_all = lax.all_gather(value_rows, 'sp', axis=1, tiled=True)  14.9 us
    all_to_all x1, waiting for transfers between devices, body(): lax.all_to_all(weights[1], 'fs', split_axis=1, concat_axis=0, tiled=True)  12.6 us
    unnamed x31, local copies, waits for them, and re-layouts  10.9 us
  transfers between devices with their start and end apart: 12, of which 9 were waited for; matrix products, arithmetic and copies ran while one was open for 22% of the time, Pallas kernels for 0%

commit v1 on v0

--- a/solution.py
+++ b/solution.py
@@ -90,7 +90,12 @@
         return lax.cond(slot <= own_index, compute, lambda states: states, carried)
 
     key_all = lax.all_gather(key_rows, "sp", axis=1, tiled=True)
-    value_all = lax.all_gather(value_rows, "sp", axis=1, tiled=True)
+    ring = [value_rows]
+    for hop in range(3):
+        ring.append(lax.ppermute(ring[-1], "sp", [(dev, (dev + 1) % 4) for dev in range(4)]))
+    value_all = jnp.roll(
+        jnp.concatenate(ring[::-1], axis=1), (lax.axis_index("sp") + 1) * ring[0].shape[1], axis=1
+    )
     blocks = key_all.shape[1] // tok_rows
 
     def turn(block_idx, states):

time: 287 us -> 287 us (level)
  blocking collectives: 60.2 us -> 44 us
  waiting for transfers between devices: 112 us -> 124 us
  local copies, waits for them, and re-layouts: 35.2 us -> 39.8 us
    all_gather x1 -> x0, blocking collectives: 14.9 us -> none  [stick_mixer(): value_all = lax.all_gather(value_rows, 'sp', axis=1, tiled=True)]
    ppermute x0 -> x3, waiting for transfers between devices: none -> 10.2 us  [stick_mixer(): lax.ppermute(ring[-1], 'sp', [(dev, (dev + 1) % 4) for dev in range(4)])]
    unnamed x31 -> x40, local copies, waits for them, and re-layouts: 10.9 us -> 12.8 us
  transfers between devices with their start and end apart: 12 -> 15, of which waited for: 9 -> 11; matrix products, arithmetic and copies ran while one was open for 22% -> 23% of each run, Pallas kernels for 0% -> 0%
where the time goes in v1:
time: 287 us; the launch traced here: 286 us
  waiting for transfers between devices  124 us (43%)
  blocking collectives  44 us (15%)
  local copies, waits for them, and re-layouts  39.8 us (14%)
  starting transfers between devices  32.9 us (11%)
  matrix products  19.8 us (7%)
  between operations  13.5 us (5%)
  other arithmetic  11.9 us (4%)
    all_gather x2, blocking collectives, carried_in(): lax.all_gather(a.astype(kind), axis)  25.9 us
    reduce_scatter x1, waiting for transfers between devices, body(): lax.psum_scatter((jnp.dot(attn_flat, full_attn, preferred_element_type=jn...  24.6 us
    all_to_all x1, waiting for transfers between devices, body(): lax.all_to_all(weights[5], 'fs', split_axis=1, concat_axis=0, tiled=True)  22.8 us
    all_to_all x1, waiting for transfers between devices, body(): lax.all_to_all(weights[4], 'fs', split_axis=1, concat_axis=0, tiled=True)  21.6 us
    all_gather x1, blocking collectives, stick_mixer(): key_all = lax.all_gather(key_rows, 'sp', axis=1, tiled=True)  15.4 us
    unnamed x40, local copies, waits for them, and re-layouts  12.8 us
    all_to_all x1, waiting for transfers between devices, body(): lax.all_to_all(weights[2], 'fs', split_axis=1, concat_axis=0, tiled=True)  12.6 us
    all_to_all x1, waiting for transfers between devices, body(): lax.all_to_all(weights[1], 'fs', split_axis=1, concat_axis=0, tiled=True)  10.6 us
  transfers between devices with their start and end apart: 15, of which 11 were waited for; matrix products, arithmetic and copies ran while one was open for 23% of the time, Pallas kernels for 0%

profile of v1, /device:TPU:0, one launch (start us, length us, event | category | flops | bytes accessed | tf_op | source)
XLA Modules:
  0.0 286.0 jit_solution(18206397352267414303)
XLA Ops:
  12.4 4.1 %all-to-all-start.4 = ((bf16[1024,2,256]{0,2,1:T(8,128)(2,1)}), bf16[1024,2,256]{0,2,1:T(8,128)(2,1)S(1)}, u32[]{:S(2)}, u32[]{:S(2)}) async-start(bf16[1024,2,256]{0,2,1:T(8,128)(2,1)} %bitcast.20), calls=%async_computation.4 | async-start | bytes 2097152 | tf_op jit(solution)/shard_map/all_to_all | solution.py:180
  17.9 21.6 %all-to-all-done.4 = bf16[1024,2,256]{0,2,1:T(8,128)(2,1)S(1)} async-done(((bf16[1024,2,256]{0,2,1:T(8,128)(2,1)}), bf16[1024,2,256]{0,2,1:T(8,128)(2,1)S(1)}, u32[]{:S(2)}, u32[]{:S(2)}) %all-to-all-start.4) | async-done | bytes 1048608 | tf_op jit(solution)/shard_map/all_to_all | solution.py:180
  39.4 3.6 %all-to-all-start.6 = ((bf16[1024,2,256]{0,2,1:T(8,128)(2,1)}), bf16[1024,2,256]{0,2,1:T(8,128)(2,1)S(1)}, u32[]{:S(2)}, u32[]{:S(2)}) async-start(bf16[1024,2,256]{0,2,1:T(8,128)(2,1)} %bitcast.29), calls=%async_computation.6 | async-start | bytes 2097152 | tf_op jit(solution)/shard_map/all_to_all | solution.py:179
  45.1 10.5 %all-to-all-done.6 = bf16[1024,2,256]{0,2,1:T(8,128)(2,1)S(1)} async-done(((bf16[1024,2,256]{0,2,1:T(8,128)(2,1)}), bf16[1024,2,256]{0,2,1:T(8,128)(2,1)S(1)}, u32[]{:S(2)}, u32[]{:S(2)}) %all-to-all-start.6) | async-done | bytes 1048608 | tf_op jit(solution)/shard_map/all_to_all | solution.py:179
  55.6 3.6 %all-to-all-start.5 = ((bf16[1024,2,256]{0,2,1:T(8,128)(2,1)}), bf16[1024,2,256]{0,2,1:T(8,128)(2,1)S(1)}, u32[]{:S(2)}, u32[]{:S(2)}) async-start(bf16[1024,2,256]{0,2,1:T(8,128)(2,1)} %bitcast.144), calls=%async_computation.5 | async-start | bytes 2097152 | tf_op jit(solution)/shard_map/all_to_all | solution.py:181
  61.5 22.8 %all-to-all-done.5 = bf16[1024,2,256]{0,2,1:T(8,128)(2,1)S(1)} async-done(((bf16[1024,2,256]{0,2,1:T(8,128)(2,1)}), bf16[1024,2,256]{0,2,1:T(8,128)(2,1)S(1)}, u32[]{:S(2)}, u32[]{:S(2)}) %all-to-all-start.5) | async-done | bytes 1048608 | tf_op jit(solution)/shard_map/all_to_all | solution.py:181
  84.4 4.4 %all-to-all-start.2 = ((bf16[1024,2,256]{0,2,1:T(8,128)(2,1)}), bf16[1024,2,256]{0,2,1:T(8,128)(2,1)}, u32[]{:S(2)}, u32[]{:S(2)}) async-start(bf16[1024,2,256]{0,2,1:T(8,128)(2,1)} %bitcast.145), calls=%async_computation.2 | async-start | bytes 2097152 | tf_op jit(solution)/shard_map/all_to_all | solution.py:178
  91.0 12.6 %all-to-all-done.2 = bf16[1024,2,256]{0,2,1:T(8,128)(2,1)} async-done(((bf16[1024,2,256]{0,2,1:T(8,128)(2,1)}), bf16[1024,2,256]{0,2,1:T(8,128)(2,1)}, u32[]{:S(2)}, u32[]{:S(2)}) %all-to-all-start.2) | async-done | bytes 1048608 | tf_op jit(solution)/shard_map/all_to_all | solution.py:178
  103.7 4.4 %all-to-all-start = ((bf16[1024,2,256]{0,2,1:T(8,128)(2,1)}), bf16[1024,2,256]{0,2,1:T(8,128)(2,1)}, u32[]{:S(2)}, u32[]{:S(2)}) async-start(bf16[1024,2,256]{0,2,1:T(8,128)(2,1)} %bitcast.146), calls=%async_computation | async-start | bytes 2097152 | tf_op jit(solution)/shard_map/all_to_all | solution.py:177
  110.4 10.6 %all-to-all-done = bf16[1024,2,256]{0,2,1:T(8,128)(2,1)} async-done(((bf16[1024,2,256]{0,2,1:T(8,128)(2,1)}), bf16[1024,2,256]{0,2,1:T(8,128)(2,1)}, u32[]{:S(2)}, u32[]{:S(2)}) %all-to-all-start) | async-done | bytes 1048608 | tf_op jit(solution)/shard_map/all_to_all | solution.py:177
  121.0 4.4 %all-to-all-start.1 = ((bf16[1024,2,256]{0,2,1:T(8,128)(2,1)}), bf16[1024,2,256]{0,2,1:T(8,128)(2,1)}, u32[]{:S(2)}, u32[]{:S(2)}) async-start(bf16[1024,2,256]{0,2,1:T(8,128)(2,1)} %bitcast.141), calls=%async_computation.1 | async-start | bytes 2097152 | tf_op jit(solution)/shard_map/all_to_all | solution.py:176
  134.2 3.3 %all-to-all-done.1 = bf16[1024,2,256]{0,2,1:T(8,128)(2,1)} async-done(((bf16[1024,2,256]{0,2,1:T(8,128)(2,1)}), bf16[1024,2,256]{0,2,1:T(8,128)(2,1)}, u32[]{:S(2)}, u32[]{:S(2)}) %all-to-all-start.1) | async-done | bytes 1048608 | tf_op jit(solution)/shard_map/all_to_all | solution.py:176
  156.9 6.9 %while.43 = (s32[]{:T(128)}, f32[2,2,128,128]{3,2,1,0:T(8,128)S(1)}, f32[2,2,2,64,128]{4,3,0,2,1:T(8,128)}, f32[2,2,2,64,128]{4,3,2,1,0:T(8,128)}, f32[2,2,2,64,...) while((s32[]{:T(128)}, ...), condition=%wide.region_11.12_spmd.clone, body=%wide.region_9.11_spmd.clone.sunk | while | flops 153571328 | bytes 3239036 | solution.py:130
  163.8 16.6 %all-gather.2 = bf16[8,2,128,128]{3,2,1,0:T(8,128)(2,1)} all-gather(bf16[2,2,128,128]{3,2,1,0:T(8,128)(2,1)S(1)} %convert_element_type.118), channel_id=4, replica_groups=mesh['grp'=2,'sp'=4,'fs'=2,'tp'=2] {'sp'}, dimensions={0}, use_global_device_ids=true | all-gather | bytes 655360 | tf_op jit(solution)/shard_map/all_gather | solution.py:18
  182.8 9.3 %all-gather.1 = bf16[8,1,2,128]{3,2,1,0:T(2,128)(2,1)S(1)} all-gather(bf16[2,1,2,128]{3,2,1,0:T(2,128)(2,1)S(1)} %slice.12), channel_id=3, replica_groups=mesh['grp'=2,'sp'=4,'fs'=2,'tp'=2] {'sp'}, dimensions={0}, use_global_device_ids=true | all-gather | bytes 5120 | tf_op jit(solution)/shard_map/all_gather | solution.py:18
  204.1 7.6 %collective-permute-done.1 = bf16[2,128,2,128]{3,1,2,0:T(8,128)(2,1)S(1)} collective-permute-done((bf16[2,128,2,128]{3,1,2,0:T(8,128)(2,1)}, bf16[2,128,2,128]{3,1,2,0:T(8,128)(2,1)S(1)}, u32[]{:S(2)}, u32[]{:S(2)}) %collective-permute-start.1) | collective-permute-done | bytes 131104 | tf_op jit(solution)/shard_map/ppermute | solution.py:95
  211.7 15.4 %all_gather.27 = bf16[2,512,2,128]{3,1,2,0:T(8,128)(2,1)S(1)} all-gather(bf16[2,128,2,128]{3,1,2,0:T(8,128)(2,1)S(1)} %copy.92), channel_id=1, replica_groups=mesh['grp'=2,'sp'=4,'fs'=2,'tp'=2] {'sp'}, dimensions={1}, use_global_device_ids=true | all-gather | bytes 655360 | tf_op jit(solution)/shard_map/all_gather | solution.py:92
  229.3 5.7 %while.42 = (s32[]{:T(128)}, f32[4,2,128,2,128]{4,2,3,1,0:T(8,128)S(1)}, f32[4,2,128,2]{2,3,1,0:T(2,128)S(1)}, s32[]{:T(128)}, bf16[2,512,2,128]{3,1,2,0:T(8,128...) while((s32[]{:T(128)}, ...), condition=%wide.region_6.7_spmd.clone, body=%wide.region_1.6_spmd.clone.sunk | while | flops 43925260 | bytes 2287439 | solution.py:106
  229.4 5.5 %conditional.3 = ((f32[4,2,128,2,128]{4,2,3,1,0:T(8,128)S(1)}, f32[4,2,128,2]{2,3,1,0:T(2,128)S(1)})) conditional(s32[]{:T(128)} %convert_element_type.168, (f32[4,2,128,2,128]{4,2,3,1,0:T(8,128)S(1)}, f32[4,2,128,2]{2,3,1,0:T(2,128)S(1)}) %tuple.100, (s32[]{:T(128)}, s32[]{:T(128)}, bf16[2,512,2,128]{3,1,2,0:T(8,128)(2,1)S(1)}, ...), branch_computations={%region_2.2_spmd, %region_3.5_spmd} | conditional | flops 43925256 | bytes 2286724 | solution.py:90
  229.9 4.4 %reduce_window_sum.43 = f32[2,2,128,128]{2,3,1,0:T(8,128)S(1)} reduce-window(f32[2,2,128,128]{2,3,1,0:T(8,128)S(1)} %get-tuple-element.514, f32[]{:T(128)} %constant.150.clone), window={size=1x1x1x128 pad=0_0x0_0x0_0x0_127}, to_apply=%region_4.3 | reduce-window | flops 8323072 | bytes 524292 | tf_op jit(solution)/shard_map/while/body/eval_jaxpr/cond/branch_1_fun/reduce_window_sum | solution.py:77
  236.2 3.4 %all-to-all-start.3 = ((bf16[2,128,256]{1,2,0:T(8,128)(2,1)}), bf16[2,128,256]{1,2,0:T(8,128)(2,1)S(1)}, u32[]{:S(2)}, u32[]{:S(2)}) async-start(bf16[2,128,256]{1,2,0:T(8,128)(2,1)} %bitcast.17), calls=%async_computation.3 | async-start | bytes 262144 | tf_op jit(solution)/shard_map/all_to_all | solution.py:216
  240.4 3.7 %all-to-all-done.3 = bf16[2,128,256]{1,2,0:T(8,128)(2,1)S(1)} async-done(((bf16[2,128,256]{1,2,0:T(8,128)(2,1)}), bf16[2,128,256]{1,2,0:T(8,128)(2,1)S(1)}, u32[]{:S(2)}, u32[]{:S(2)}) %all-to-all-start.3) | async-done | bytes 131104 | tf_op jit(solution)/shard_map/all_to_all | solution.py:216
  244.1 3.4 %all-to-all-start.7 = ((bf16[2,128,256]{1,2,0:T(8,128)(2,1)}), bf16[2,128,256]{1,2,0:T(8,128)(2,1)S(1)}, u32[]{:S(2)}, u32[]{:S(2)}) async-start(bf16[2,128,256]{1,2,0:T(8,128)(2,1)} %bitcast.38), calls=%async_computation.7 | async-start | bytes 262144 | tf_op jit(solution)/shard_map/all_to_all | solution.py:217
  254.8 24.6 %reduce-scatter.2.cloned.1.call-done = bf16[64,2048]{1,0:T(8,128)(2,1)} async-done(((bf16[128,2048]{1,0:T(8,128)(2,1)}), bf16[64,2048]{1,0:T(8,128)(2,1)}) %reduce-scatter.2.cloned.1.call-update) | async-done | bytes 262160 | tf_op jit(solution)/shard_map/reduce_scatter | solution.py:224
  (139 shorter events, 77.6 us)
Async XLA Ops:
  6.5 119.8 %copy-start = (f32[4,128]{1,0:T(4,128)S(1)}, f32[4,128]{1,0:T(4,128)}, u32[]{:S(2)}) copy-start(f32[4,128]{1,0:T(4,128)} %param.30) | copy-start | bytes 6148
  6.5 133.3 %all-gather.11.cloned.1.call-start = ((), (), s32[]{:S(2)}) async-start(), calls=%async_computation.12 | async-start | bytes 1572864 | tf_op jit(solution)/shard_map/all_gather | solution.py:183
  11.1 5.5 %copy-start.6 = (bf16[1024,512]{1,0:T(8,128)(2,1)S(1)}, bf16[1024,512]{1,0:T(8,128)(2,1)}, u32[]{:S(2)}) copy-start(bf16[1024,512]{1,0:T(8,128)(2,1)} %param.26) | copy-start | bytes 3145732
  12.4 27.0 %all-to-all-start.4 = ((bf16[1024,2,256]{0,2,1:T(8,128)(2,1)}), bf16[1024,2,256]{0,2,1:T(8,128)(2,1)S(1)}, u32[]{:S(2)}, u32[]{:S(2)}) async-start(bf16[1024,2,256]{0,2,1:T(8,128)(2,1)} %bitcast.20), calls=%async_computation.4 | async-start | bytes 2097152 | tf_op jit(solution)/shard_map/all_to_all | solution.py:180
  17.9 25.9 %copy-start.7 = (bf16[1024,512]{1,0:T(8,128)(2,1)S(1)}, bf16[1024,512]{1,0:T(8,128)(2,1)}, u32[]{:S(2)}) copy-start(bf16[1024,512]{1,0:T(8,128)(2,1)} %param.28) | copy-start | bytes 3145732
  39.4 16.2 %all-to-all-start.6 = ((bf16[1024,2,256]{0,2,1:T(8,128)(2,1)}), bf16[1024,2,256]{0,2,1:T(8,128)(2,1)S(1)}, u32[]{:S(2)}, u32[]{:S(2)}) async-start(bf16[1024,2,256]{0,2,1:T(8,128)(2,1)} %bitcast.29), calls=%async_computation.6 | async-start | bytes 2097152 | tf_op jit(solution)/shard_map/all_to_all | solution.py:179
  43.0 204.5 %all-gather.7.cloned.1.call-start = ((), (), s32[]{:S(2)}) async-start(), calls=%async_computation.9 | async-start | bytes 3145728 | tf_op jit(solution)/shard_map/all_gather | solution.py:220
  55.6 28.7 %all-to-all-start.5 = ((bf16[1024,2,256]{0,2,1:T(8,128)(2,1)}), bf16[1024,2,256]{0,2,1:T(8,128)(2,1)S(1)}, u32[]{:S(2)}, u32[]{:S(2)}) async-start(bf16[1024,2,256]{0,2,1:T(8,128)(2,1)} %bitcast.144), calls=%async_computation.5 | async-start | bytes 2097152 | tf_op jit(solution)/shard_map/all_to_all | solution.py:181
  84.4 19.3 %all-to-all-start.2 = ((bf16[1024,2,256]{0,2,1:T(8,128)(2,1)}), bf16[1024,2,256]{0,2,1:T(8,128)(2,1)}, u32[]{:S(2)}, u32[]{:S(2)}) async-start(bf16[1024,2,256]{0,2,1:T(8,128)(2,1)} %bitcast.145), calls=%async_computation.2 | async-start | bytes 2097152 | tf_op jit(solution)/shard_map/all_to_all | solution.py:178
  103.7 17.3 %all-to-all-start = ((bf16[1024,2,256]{0,2,1:T(8,128)(2,1)}), bf16[1024,2,256]{0,2,1:T(8,128)(2,1)}, u32[]{:S(2)}, u32[]{:S(2)}) async-start(bf16[1024,2,256]{0,2,1:T(8,128)(2,1)} %bitcast.146), calls=%async_computation | async-start | bytes 2097152 | tf_op jit(solution)/shard_map/all_to_all | solution.py:177
  110.4 15.8 %copy-start.12 = (f32[4]{0:T(128)S(1)}, f32[4]{0:T(128)}, u32[]{:S(2)}) copy-start(f32[4]{0:T(128)} %param.29) | copy-start | bytes 52
  121.0 16.5 %all-to-all-start.1 = ((bf16[1024,2,256]{0,2,1:T(8,128)(2,1)}), bf16[1024,2,256]{0,2,1:T(8,128)(2,1)}, u32[]{:S(2)}, u32[]{:S(2)}) async-start(bf16[1024,2,256]{0,2,1:T(8,128)(2,1)} %bitcast.141), calls=%async_computation.1 | async-start | bytes 2097152 | tf_op jit(solution)/shard_map/all_to_all | solution.py:176
  125.4 126.5 %all-gather.9.cloned.1.call-start = ((), (), s32[]{:S(2)}) async-start(), calls=%async_computation.10 | async-start | bytes 3145728 | tf_op jit(solution)/shard_map/all_gather | solution.py:221
  132.6 7.2 %copy-start.8 = (bf16[2,1024,256]{2,1,0:T(8,128)(2,1)S(1)}, bf16[2,1024,256]{2,1,0:T(8,128)(2,1)}, u32[]{:S(2)}) copy-start(bf16[2,1024,256]{2,1,0:T(8,128)(2,1)} %copy.103) | copy-start | bytes 3145732
  139.8 6.2 %copy-start.1 = (bf16[1,256,2048]{2,1,0:T(8,128)(2,1)S(1)}, bf16[1,256,2048]{2,1,0:T(8,128)(2,1)}, u32[]{:S(2)}) copy-start(bf16[1,256,2048]{2,1,0:T(8,128)(2,1)} %all-gather.11.cloned.1.call-done) | copy-start | bytes 3145732
  144.1 7.8 %copy-start.4 = (bf16[2,1024,256]{2,1,0:T(8,128)(2,1)S(1)}, bf16[2,1024,256]{2,1,0:T(8,128)(2,1)}, u32[]{:S(2)}) copy-start(bf16[2,1024,256]{2,1,0:T(8,128)(2,1)} %copy.106) | copy-start | bytes 3145732
  195.1 5.2 %copy-start.2 = (bf16[2,1024,256]{2,1,0:T(8,128)(2,1)S(1)}, bf16[2,1024,256]{2,1,0:T(8,128)(2,1)}, u32[]{:S(2)}) copy-start(bf16[2,1024,256]{2,1,0:T(8,128)(2,1)} %copy.94) | copy-start | bytes 3145732
  196.8 7.3 %collective-permute-start = (bf16[2,128,2,128]{3,1,2,0:T(8,128)(2,1)}, bf16[2,128,2,128]{3,1,2,0:T(8,128)(2,1)}, u32[]{:S(2)}, u32[]{:S(2)}) collective-permute-start(bf16[2,128,2,128]{3,1,2,0:T(8,128)(2,1)} %copy.97), channel_id=1, source_target_pairs={{0,4},{4,8},{8,12},{12,0},{1,5},{5,9},{9,13},{13,1},{2,6},{6,10},{... | collective-permute-start | bytes 393224 | tf_op jit(solution)/shard_map/ppermute | solution.py:95
  204.1 7.6 %collective-permute-start.1 = (bf16[2,128,2,128]{3,1,2,0:T(8,128)(2,1)}, bf16[2,128,2,128]{3,1,2,0:T(8,128)(2,1)S(1)}, u32[]{:S(2)}, u32[]{:S(2)}) collective-permute-start(bf16[2,128,2,128]{3,1,2,0:T(8,128)(2,1)} %collective-permute-done), channel_id=1, source_target_pairs={{0,4},{4,8},{8,12},{12,0},{1,5},{5,9},{9,13},{13,1},{2,6},{6,10},{... | collective-permute-start | bytes 393224 | tf_op jit(solution)/shard_map/ppermute | solution.py:95
  211.7 15.4 %collective-permute-start.2 = (bf16[2,128,2,128]{3,1,2,0:T(8,128)(2,1)S(1)}, bf16[2,128,2,128]{3,1,2,0:T(8,128)(2,1)S(1)}, u32[]{:S(2)}, u32[]{:S(2)}) collective-permute-start(bf16[2,128,2,128]{3,1,2,0:T(8,128)(2,1)S(1)} %collective-permute-done.1), channel_id=1, source_target_pairs={{0,4},{4,8},{8,12},{12,0},{1,5},{5,9},{9,13},{13,1},{2,6},{6,10},{... | collective-permute-start | bytes 393224 | tf_op jit(solution)/shard_map/ppermute | solution.py:95
  229.3 10.3 %copy-start.11 = (f32[128]{0:T(128)S(1)}, f32[128]{0:T(128)}, u32[]{:S(2)}) copy-start(f32[128]{0:T(128)} %param.31) | copy-start | bytes 1540
  236.2 7.8 %all-to-all-start.3 = ((bf16[2,128,256]{1,2,0:T(8,128)(2,1)}), bf16[2,128,256]{1,2,0:T(8,128)(2,1)S(1)}, u32[]{:S(2)}, u32[]{:S(2)}) async-start(bf16[2,128,256]{1,2,0:T(8,128)(2,1)} %bitcast.17), calls=%async_computation.3 | async-start | bytes 262144 | tf_op jit(solution)/shard_map/all_to_all | solution.py:216
  244.1 7.8 %all-to-all-start.7 = ((bf16[2,128,256]{1,2,0:T(8,128)(2,1)}), bf16[2,128,256]{1,2,0:T(8,128)(2,1)S(1)}, u32[]{:S(2)}, u32[]{:S(2)}) async-start(bf16[2,128,256]{1,2,0:T(8,128)(2,1)} %bitcast.38), calls=%async_computation.7 | async-start | bytes 262144 | tf_op jit(solution)/shard_map/all_to_all | solution.py:217
  247.5 32.0 %reduce-scatter.2.cloned.1.call-start = ((), (), s32[]{:S(2)}) async-start(), calls=%async_computation.11 | async-start | bytes 786432 | tf_op jit(solution)/shard_map/reduce_scatter | solution.py:224
  (4 other events, 9.6 us)
Sparse Core Ops, SparseCore 0:
  11.2 31.5 all-gather.10
  45.4 49.9 all-gather.6
  127.8 34.1 all-gather.8
  254.9 24.4 reduce-scatter.1
